TPU v7x, 32 devices: a whole 2x2x4 slice. The times are simulated.
32 devices in a mesh: sp: 8 (over z, y), tp: 4 (over x, core).
Axes of the slice: x: 2, y: 2, z: 4, core: 2. Of those that a mesh axis runs over, the one named last changes fastest.
Arguments:
- q_proj: bfloat16 [4096, 1024], P('sp', 'tp'), may hold values from -5.25 to 5.25
- k_proj: bfloat16 [4096, 512], P('sp', 'tp'), may hold values from -5.25 to 5.25
- v_proj: bfloat16 [4096, 512], P('sp', 'tp'), may hold values from -6 to 6
- doc_ids: int32 [4096], P('sp'), may hold values from 0 to 3, never falling along the last dimension, each value on 1 to 2048 neighbouring positions
- sinks: float32 [16], P('tp'), may hold values from 0.5 to 5.5
- resid: bfloat16 [4096, 2048], P(('sp', 'tp')), may hold values from -12 to 12
- w_out: bfloat16 [1024, 2048], P('tp'), may hold values from -4 to 4
- norm_gain: float32 [2048], replicated, may hold values from 0.1 to 1.9
- w_gate: bfloat16 [2048, 5632], P('sp', 'tp'), may hold values from -0.125 to 0.125
- w_up: bfloat16 [2048, 5632], P('sp', 'tp'), may hold values from -0.125 to 0.125
- w_down: bfloat16 [5632, 2048], P('tp', 'sp'), may hold values from -0.078125 to 0.078125
Outputs:
- layer_out: bfloat16 [4096, 2048], P(('sp', 'tp'))
Inputs may be any that keep to these rules, and one draw needn't show every extreme that they name: `doc_ids`: document numbers never fall along the sequence; each document covers at most 2048 positions and one covers exactly that many.
All inputs are finite; a program needn't handle non-finite values.
Results may differ from a plain program's by a relative error of at most 0.015.
Values may be sent and summed in bfloat16 or wider, within the bound.
No kernel may reach another device: no remote copies, remote signals or barrier semaphores. Data moves between devices by JAX's collectives and lax.ppermute only.
A program may use at most 64 MiB of HBM per device.

v0:
```python
import jax
import jax.numpy as jnp
from jax import lax
from jax.sharding import PartitionSpec as P

HEAD = 64
WINDOW = 128
norm_eps = 1e-06
masked = -1e30


def with_halo(block, sides, width):
    for axis, dim in sides:
        count = lax.axis_size(axis)
        forward = [(i, i + 1) for i in range(count - 1)]
        backward = [(target, source) for source, target in forward]
        low = lax.ppermute(
            lax.slice_in_dim(block, block.shape[dim] - width, None, axis=dim), axis, forward
        )
        high = lax.ppermute(lax.slice_in_dim(block, 0, width, axis=dim), axis, backward)
        block = jnp.concatenate([low, block, high], axis=dim)
    return block


def normalize(middle, norm_gain):
    return (
        middle * lax.rsqrt(jnp.mean(middle * middle, axis=-1, keepdims=True) + norm_eps) * norm_gain
    ).astype(jnp.bfloat16)


def band_view(extended, block_count):
    shaped = extended.reshape((block_count + 2, WINDOW) + extended.shape[1:])
    return jnp.concatenate([shaped[:-2], shaped[1:-1], shaped[2:]], axis=1)


def shards(q_proj, k_proj, v_proj, doc_ids, sinks, resid, w_out, norm_gain, w_gate, w_up, w_down):
    tok_rows = q_proj.shape[0]
    kv_local = k_proj.shape[1] // HEAD
    groups = q_proj.shape[1] // HEAD // kv_local
    block_count = tok_rows // WINDOW
    full_out = lax.all_gather(w_out, "tp", axis=0, tiled=True)
    keys_ext, values_ext, docs_ext = (
        with_halo(k_proj, (("sp", 0),), WINDOW),
        with_halo(v_proj, (("sp", 0),), WINDOW),
        with_halo(doc_ids, (("sp", 0),), WINDOW),
    )
    positions = (
        lax.axis_index("sp") * tok_rows
        - WINDOW
        + jnp.arange(tok_rows + 2 * WINDOW, dtype=jnp.int32)
    )
    inside = (positions >= 0) & (positions < tok_rows * lax.axis_size("sp"))
    docs_ext = jnp.where(inside, docs_ext, -1)
    key_band = band_view(keys_ext.reshape(tok_rows + 2 * WINDOW, kv_local, HEAD), block_count)
    value_band = band_view(values_ext.reshape(tok_rows + 2 * WINDOW, kv_local, HEAD), block_count)
    doc_band = band_view(docs_ext, block_count)
    queries = q_proj.reshape(block_count, WINDOW, kv_local, groups, HEAD)
    scores = jnp.einsum(
        "bqhgd,bkhd->bhgqk", queries, key_band, preferred_element_type=jnp.float32
    ) * HEAD ** (-0.5)
    offsets = jnp.arange(3 * WINDOW, dtype=jnp.int32) - WINDOW
    near = jnp.abs(jnp.arange(WINDOW, dtype=jnp.int32)[:, None] - offsets[None, :]) <= WINDOW
    query_docs = doc_ids.reshape(block_count, WINDOW)
    valid = near[None] & (query_docs[:, :, None] == doc_band[:, None, :])
    scores = jnp.where(valid[:, None, None], scores, masked)
    sink_table = sinks.reshape(kv_local, groups)[None, :, :, None, None]
    top = jnp.maximum(jnp.max(scores, axis=-1, keepdims=True), sink_table)
    expd = jnp.exp(scores - top)
    probs = (expd / (jnp.sum(expd, axis=-1, keepdims=True) + jnp.exp(sink_table - top))).astype(
        jnp.bfloat16
    )
    attended = jnp.einsum(
        "bhgqk,bkhd->bqhgd", probs, value_band, preferred_element_type=jnp.float32
    )
    attended = attended.astype(jnp.bfloat16).reshape(tok_rows, kv_local * groups * HEAD)
    own_rows = lax.all_to_all(attended, "tp", split_axis=0, concat_axis=1, tiled=True)
    projected = jnp.dot(own_rows, full_out, preferred_element_type=jnp.float32)
    middle = resid.astype(jnp.float32) + projected
    normed = lax.all_gather(normalize(middle, norm_gain), "tp", axis=0, tiled=True)

    def add_rows(piece):
        return jnp.dot(normed, piece, preferred_element_type=jnp.float32)

    gate = add_rows(lax.all_gather(w_gate, "sp", axis=0, tiled=True))
    up_part = add_rows(lax.all_gather(w_up, "sp", axis=0, tiled=True))
    hidden = (jax.nn.silu(gate) * up_part).astype(jnp.bfloat16)
    down_full = lax.all_gather(w_down, "sp", axis=1, tiled=True)
    summed_down = lax.psum_scatter(
        jnp.dot(hidden, down_full, preferred_element_type=jnp.float32).astype(jnp.bfloat16),
        "tp",
        scatter_dimension=0,
        tiled=True,
    ).astype(jnp.float32)
    return (middle + summed_down).astype(jnp.bfloat16)


def solution(mesh):
    placed = (
        P("sp", "tp"),
        P("sp", "tp"),
        P("sp", "tp"),
        P("sp"),
        P("tp"),
        P(("sp", "tp"), None),
        P("tp", None),
        P(),
        P("sp", "tp"),
        P("sp", "tp"),
        P("tp", "sp"),
    )
    return jax.shard_map(
        shards, mesh=mesh, in_specs=placed, out_specs=P(("sp", "tp"), None), check_vma=False
    )
```

profile of v0, /device:TPU:0, one launch (start us, length us, event | category | flops | bytes accessed | tf_op | source)
XLA Modules:
  0.0 408.3 jit_solution(3084332801912330174)
XLA Ops:
  6.6 0.7 all-gather.6.cloned.1.call-update
  7.3 0.8 fusion.27
  8.1 4.9 %collective-permute-start.2 = (s32[128]{0:T(128)S(1)}, s32[128]{0:T(128)S(1)}, u32[]{:S(2)}, u32[]{:S(2)}) collective-permute-start(s32[128]{0:T(128)S(1)} %get-tuple-element.16), channel_id=1, source_target_pairs={{0,4},{4,8},{8,12},{12,16},{16,20},{20,24},{24,28},{1,5},{5,9},{9,... | collective-permute-start | bytes 1544 | tf_op jit(solution)/shard_map/ppermute | solution.py:17
  13.0 1.3 collective-permute-start.3
  14.3 0.8 fusion.25
  15.1 4.5 %collective-permute-start.4 = (bf16[128,128]{1,0:T(8,128)(2,1)S(1)}, bf16[128,128]{1,0:T(8,128)(2,1)S(1)}, u32[]{:S(2)}, u32[]{:S(2)}) collective-permute-start(bf16[128,128]{1,0:T(8,128)(2,1)S(1)} %get-tuple-element.11), channel_id=1, source_target_pairs={{0,4},{4,8},{8,12},{12,16},{16,20},{20,24},{24,28},{1,5},{5,9},{9,... | collective-permute-start | bytes 98312 | tf_op jit(solution)/shard_map/ppermute | solution.py:17
  19.6 1.3 collective-permute-start.5
  20.9 0.8 fusion.24
  21.7 4.9 %collective-permute-start = (bf16[128,128]{1,0:T(8,128)(2,1)S(1)}, bf16[128,128]{1,0:T(8,128)(2,1)S(1)}, u32[]{:S(2)}, u32[]{:S(2)}) collective-permute-start(bf16[128,128]{1,0:T(8,128)(2,1)S(1)} %get-tuple-element.7), channel_id=1, source_target_pairs={{0,4},{4,8},{8,12},{12,16},{16,20},{20,24},{24,28},{1,5},{5,9},{9,... | collective-permute-start | bytes 98312 | tf_op jit(solution)/shard_map/ppermute | solution.py:17
  26.6 1.0 reshape.90
  27.7 1.0 reshape.87
  28.9 1.2 reshape.92
  30.5 1.3 collective-permute-start.1
  31.9 0.3 compare_and_fusion
  32.8 4.4 %collective-permute-done.1 = bf16[128,128]{1,0:T(8,128)(2,1)S(1)} collective-permute-done((bf16[128,128]{1,0:T(8,128)(2,1)S(1)}, bf16[128,128]{1,0:T(8,128)(2,1)S(1)}, u32[]{:S(2)}, u32[]{:S(2)}) %collective-permute-start.1) | collective-permute-done | bytes 32800 | tf_op jit(solution)/shard_map/ppermute | solution.py:20
  37.8 0.7 fusion.2
  38.6 0.7 fusion.1
  39.4 1.0 fusion.4
  40.4 8.6 %all_to_all.19 = bf16[4,128,256]{1,2,0:T(8,128)(2,1)S(1)} all-to-all(bf16[4,128,256]{1,2,0:T(8,128)(2,1)S(1)} %bitcast.42), channel_id=1, replica_groups=mesh['sp'=8,'tp'=4] {'tp'}, dimensions={0} | all-to-all | bytes 524288 | tf_op jit(solution)/shard_map/all_to_all | solution.py:76
  49.0 3.0 multiply_reduce_fusion
  52.0 1.0 multiply_convert_fusion
  53.0 0.7 all-gather.10.cloned.1.call-update
  53.7 0.5 all-gather.12.cloned.1.call-update
  54.3 0.5 all-gather.14.cloned.1.call-update
  55.1 21.3 %all-gather.8.cloned.1.call-done = bf16[512,2048]{1,0:T(8,128)(2,1)} async-done(((bf16[128,2048]{1,0:T(8,128)(2,1)}), bf16[512,2048]{1,0:T(8,128)(2,1)}) %all-gather.8.cloned.1.call-update) | async-done | bytes 2097168 | tf_op jit(solution)/shard_map/all_gather | solution.py:79
  76.4 94.5 %all-gather.10.cloned.1.call-done = bf16[2048,1408]{1,0:T(8,128)(2,1)} async-done(((bf16[256,1408]{1,0:T(8,128)(2,1)}), bf16[2048,1408]{1,0:T(8,128)(2,1)}) %all-gather.10.cloned.1.call-update) | async-done | bytes 5767184 | tf_op jit(solution)/shard_map/all_gather | solution.py:84
  170.9 8.3 %fusion.28 = f32[512,1408]{1,0:T(8,128)} fusion(bf16[512,2048]{1,0:T(8,128)(2,1)} %all-gather.8.cloned.1.call-done, bf16[2048,1408]{1,0:T(8,128)(2,1)} %all-gather.10.cloned.1.call-done), kind=kOutput, calls=%fused_computation.52 | convolution fusion | flops 2952790016 | bytes 10747904 | tf_op jit(solution)/shard_map/dot_general | solution.py:82
  179.2 84.3 %all-gather.12.cloned.1.call-done = bf16[2048,1408]{1,0:T(8,128)(2,1)} async-done(((bf16[256,1408]{1,0:T(8,128)(2,1)}), bf16[2048,1408]{1,0:T(8,128)(2,1)}) %all-gather.12.cloned.1.call-update) | async-done | bytes 5767184 | tf_op jit(solution)/shard_map/all_gather | solution.py:85
  263.5 93.2 %all-gather.14.cloned.1.call-done = bf16[1408,2048]{1,0:T(8,128)(2,1)} async-done(((bf16[1408,256]{1,0:T(8,128)(2,1)}), bf16[1408,2048]{1,0:T(8,128)(2,1)}) %all-gather.14.cloned.1.call-update) | async-done | bytes 5767184 | tf_op jit(solution)/shard_map/all_gather | solution.py:87
  356.7 13.3 %convolution_convert_fusion = bf16[512,2048]{1,0:T(8,128)(2,1)} fusion(bf16[1408,2048]{1,0:T(8,128)(2,1)} %all-gather.14.cloned.1.call-done, bf16[512,2048]{1,0:T(8,128)(2,1)S(1)} %copy-done.5, bf16[2048,1408]{1,0:T(8,128)(2,1)} %all-gather.12.cloned.1.call-done, f32[512,1408]{1,0:T(8,128)} %fusion.28), kind=kOutput, calls=%fused_computation.5 | convolution fusion | flops 5910953984 | bytes 18612224 | tf_op jit(solution)/shard_map/dot_general | solution.py:89
  370.0 29.5 %reduce-scatter.2.cloned.1.call-done = bf16[128,2048]{1,0:T(8,128)(2,1)} async-done(((bf16[512,2048]{1,0:T(8,128)(2,1)}), bf16[128,2048]{1,0:T(8,128)(2,1)}) %reduce-scatter.2.cloned.1.call-update) | async-done | bytes 524304 | tf_op jit(solution)/shard_map/reduce_scatter | solution.py:88
  399.5 1.9 add_convert_fusion
  (49 shorter events, 2.3 us)
Async XLA Ops:
  6.5 25.3 %copy-start.3 = (s32[512]{0:T(512)S(1)}, s32[512]{0:T(512)}, u32[]{:S(2)}) copy-start(s32[512]{0:T(512)} %param.14) | copy-start | bytes 6148
  6.5 25.6 %copy-start = (bf16[512,128]{1,0:T(8,128)(2,1)S(1)}, bf16[512,128]{1,0:T(8,128)(2,1)}, u32[]{:S(2)}) copy-start(bf16[512,128]{1,0:T(8,128)(2,1)} %param.12) | copy-start | bytes 393220
  6.5 30.7 %copy-start.1 = (bf16[512,128]{1,0:T(8,128)(2,1)S(1)}, bf16[512,128]{1,0:T(8,128)(2,1)}, u32[]{:S(2)}) copy-start(bf16[512,128]{1,0:T(8,128)(2,1)} %param.13) | copy-start | bytes 393220
  6.5 23.7 %copy-start.6 = (f32[4]{0:T(128)S(1)}, f32[4]{0:T(128)}, u32[]{:S(2)}) copy-start(f32[4]{0:T(128)} %param.15) | copy-start | bytes 52
  6.5 42.4 %all-gather.6.cloned.1.call-start = ((), (), s32[]{:S(2)}) async-start(), calls=%async_computation.2 | async-start | bytes 5242880 | tf_op jit(solution)/shard_map/all_gather | solution.py:41
  7.3 69.1 %all-gather.8.cloned.1.call-start = ((), (), s32[]{:S(2)}) async-start(), calls=%async_computation.3 | async-start | bytes 2621440 | tf_op jit(solution)/shard_map/all_gather | solution.py:79
  8.1 22.4 %collective-permute-start.2 = (s32[128]{0:T(128)S(1)}, s32[128]{0:T(128)S(1)}, u32[]{:S(2)}, u32[]{:S(2)}) collective-permute-start(s32[128]{0:T(128)S(1)} %get-tuple-element.16), channel_id=1, source_target_pairs={{0,4},{4,8},{8,12},{12,16},{16,20},{20,24},{24,28},{1,5},{5,9},{9,... | collective-permute-start | bytes 1544 | tf_op jit(solution)/shard_map/ppermute | solution.py:17
  13.0 18.8 %collective-permute-start.3 = (s32[128]{0:T(128)S(1)}, s32[128]{0:T(128)S(1)}, u32[]{:S(2)}, u32[]{:S(2)}) collective-permute-start(s32[128]{0:T(128)S(1)} %get-tuple-element.17), channel_id=1, source_target_pairs={{4,0},{8,4},{12,8},{16,12},{20,16},{24,20},{28,24},{5,1},{9,5},{13... | collective-permute-start | bytes 1544 | tf_op jit(solution)/shard_map/ppermute | solution.py:20
  15.1 17.1 %collective-permute-start.4 = (bf16[128,128]{1,0:T(8,128)(2,1)S(1)}, bf16[128,128]{1,0:T(8,128)(2,1)S(1)}, u32[]{:S(2)}, u32[]{:S(2)}) collective-permute-start(bf16[128,128]{1,0:T(8,128)(2,1)S(1)} %get-tuple-element.11), channel_id=1, source_target_pairs={{0,4},{4,8},{8,12},{12,16},{16,20},{20,24},{24,28},{1,5},{5,9},{9,... | collective-permute-start | bytes 98312 | tf_op jit(solution)/shard_map/ppermute | solution.py:17
  19.6 12.6 %collective-permute-start.5 = (bf16[128,128]{1,0:T(8,128)(2,1)S(1)}, bf16[128,128]{1,0:T(8,128)(2,1)S(1)}, u32[]{:S(2)}, u32[]{:S(2)}) collective-permute-start(bf16[128,128]{1,0:T(8,128)(2,1)S(1)} %get-tuple-element.12), channel_id=1, source_target_pairs={{4,0},{8,4},{12,8},{16,12},{20,16},{24,20},{28,24},{5,1},{9,5},{13... | collective-permute-start | bytes 98312 | tf_op jit(solution)/shard_map/ppermute | solution.py:20
  21.7 11.1 %collective-permute-start = (bf16[128,128]{1,0:T(8,128)(2,1)S(1)}, bf16[128,128]{1,0:T(8,128)(2,1)S(1)}, u32[]{:S(2)}, u32[]{:S(2)}) collective-permute-start(bf16[128,128]{1,0:T(8,128)(2,1)S(1)} %get-tuple-element.7), channel_id=1, source_target_pairs={{0,4},{4,8},{8,12},{12,16},{16,20},{20,24},{24,28},{1,5},{5,9},{9,... | collective-permute-start | bytes 98312 | tf_op jit(solution)/shard_map/ppermute | solution.py:17
  30.5 6.7 %collective-permute-start.1 = (bf16[128,128]{1,0:T(8,128)(2,1)S(1)}, bf16[128,128]{1,0:T(8,128)(2,1)S(1)}, u32[]{:S(2)}, u32[]{:S(2)}) collective-permute-start(bf16[128,128]{1,0:T(8,128)(2,1)S(1)} %get-tuple-element.8), channel_id=1, source_target_pairs={{4,0},{8,4},{12,8},{16,12},{20,16},{24,20},{28,24},{5,1},{9,5},{13... | collective-permute-start | bytes 98312 | tf_op jit(solution)/shard_map/ppermute | solution.py:20
  39.4 9.6 %copy-start.2 = (bf16[128,2048]{1,0:T(8,128)(2,1)S(1)}, bf16[128,2048]{1,0:T(8,128)(2,1)}, u32[]{:S(2)}) copy-start(bf16[128,2048]{1,0:T(8,128)(2,1)} %param.16) | copy-start | bytes 1572868
  48.9 3.0 copy-start.4
  53.0 117.9 %all-gather.10.cloned.1.call-start = ((), (), s32[]{:S(2)}) async-start(), calls=%async_computation.4 | async-start | bytes 6488064 | tf_op jit(solution)/shard_map/all_gather | solution.py:84
  53.7 209.8 %all-gather.12.cloned.1.call-start = ((), (), s32[]{:S(2)}) async-start(), calls=%async_computation.5 | async-start | bytes 6488064 | tf_op jit(solution)/shard_map/all_gather | solution.py:85
  54.3 302.4 %all-gather.14.cloned.1.call-start = ((), (), s32[]{:S(2)}) async-start(), calls=%async_computation.6 | async-start | bytes 6488064 | tf_op jit(solution)/shard_map/all_gather | solution.py:87
  54.9 344.6 %reduce-scatter.2.cloned.1.call-start = ((), (), s32[]{:S(2)}) async-start(), calls=%async_computation.7 | async-start | bytes 2621440 | tf_op jit(solution)/shard_map/reduce_scatter | solution.py:88
  76.4 280.3 %copy-start.5 = (bf16[512,2048]{1,0:T(8,128)(2,1)S(1)}, bf16[512,2048]{1,0:T(8,128)(2,1)}, u32[]{:S(2)}) copy-start(bf16[512,2048]{1,0:T(8,128)(2,1)} %all-gather.8.cloned.1.call-done) | copy-start | bytes 6291460
Sparse Core Ops, SparseCore 0:
  8.9 37.1 all-gather.5
  53.1 23.2 all-gather.7
  78.5 92.3 all-gather.9
  172.9 90.4 all-gather.11
  265.3 91.2 all-gather.13
  370.1 29.3 reduce-scatter.1
where the time goes:
time: 409 us; the launch traced here: 408 us
  waiting for transfers between devices  330 us (81%)
  matrix products  26.2 us (6%)
  starting transfers between devices  18.6 us (5%)
  between operations  13.8 us (3%)
  blocking collectives  8.59 us (2%)
  local copies, waits for them, and re-layouts  7.14 us (2%)
  other arithmetic  4.2 us (1%)
    all_gather x1, waiting for transfers between devices, shards(): gate = add_rows(lax.all_gather(w_gate, 'sp', axis=0, tiled=True))  94.5 us
    all_gather x1, waiting for transfers between devices, shards(): down_full = lax.all_gather(w_down, 'sp', axis=1, tiled=True)  93.2 us
    all_gather x1, waiting for transfers between devices, shards(): up_part = add_rows(lax.all_gather(w_up, 'sp', axis=0, tiled=True))  84.3 us
    reduce_scatter x1, waiting for transfers between devices, shards(): lax.psum_scatter(jnp.dot(hidden, down_full, preferred_element_type=jnp.fl...  29.5 us
    all_gather x1, waiting for transfers between devices, shards(): lax.all_gather(normalize(middle, norm_gain), 'tp', axis=0, tiled=True)  21.3 us
    ppermute x3, starting transfers between devices, with_halo(): lax.ppermute(lax.slice_in_dim(block, block.shape[dim] - width, None, axis...  14.4 us
    dot_general x1, matrix products, shards(): jnp.dot(hidden, down_full, preferred_element_type=jnp.float32)  13.3 us
    all_to_all x1, blocking collectives, shards(): lax.all_to_all(attended, 'tp', split_axis=0, concat_axis=1, tiled=True)  8.59 us
  transfers between devices with their start and end apart: 12, of which 6 were waited for; matrix products, arithmetic and copies ran while one was open for 4% of the time, Pallas kernels for 0%

commit v1 on v0

--- a/solution.py
+++ b/solution.py
@@ -84,7 +84,13 @@
     gate = add_rows(lax.all_gather(w_gate, "sp", axis=0, tiled=True))
     up_part = add_rows(lax.all_gather(w_up, "sp", axis=0, tiled=True))
     hidden = (jax.nn.silu(gate) * up_part).astype(jnp.bfloat16)
-    down_full = lax.all_gather(w_down, "sp", axis=1, tiled=True)
+    size = lax.axis_size("sp")
+    current, parts = (w_down, [w_down])
+    for _ in range(size - 1):
+        current = lax.ppermute(current, "sp", [(i_2, (i_2 + 1) % size) for i_2 in range(size)])
+        parts.insert(0, current)
+    flat = jnp.concatenate(parts, axis=1)
+    down_full = jnp.roll(flat, (lax.axis_index("sp") + 1) * w_down.shape[1], axis=1)
     summed_down = lax.psum_scatter(
         jnp.dot(hidden, down_full, preferred_element_type=jnp.float32).astype(jnp.bfloat16),
         "tp",

time: 409 us -> 374 us (0.914)
  waiting for transfers between devices: 330 us -> 262 us
  local copies, waits for them, and re-layouts: 7.14 us -> 32.8 us
    ppermute x0 -> x7, waiting for transfers between devices: none -> 191 us  [shards(): lax.ppermute(current, 'sp', [(i_2, (i_2 + 1) % size) for i_2 in range(siz...]
    all_gather x1, waiting for transfers between devices: 94.5 us -> 0.01 us  [shards(): gate = add_rows(lax.all_gather(w_gate, 'sp', axis=0, tiled=True))]
    all_gather x1 -> x0, waiting for transfers between devices: 93.2 us -> none  [shards(): down_full = lax.all_gather(w_down, 'sp', axis=1, tiled=True)]
    all_gather x1, waiting for transfers between devices: 84.3 us -> 38.1 us  [shards(): up_part = add_rows(lax.all_gather(w_up, 'sp', axis=0, tiled=True))]
    unnamed x14 -> x37, local copies, waits for them, and re-layouts: 0.03 us -> 24 us
    all_gather x1, waiting for transfers between devices: 21.3 us -> 0.01 us  [shards(): lax.all_gather(normalize(middle, norm_gain), 'tp', axis=0, tiled=True)]
  transfers between devices with their start and end apart: 12 -> 18, of which waited for: 6 -> 10; matrix products, arithmetic and copies ran while one was open for 4% -> 12% of each run, Pallas kernels for 0% -> 0%
where the time goes in v1:
time: 374 us; the launch traced here: 373 us
  waiting for transfers between devices  262 us (70%)
  local copies, waits for them, and re-layouts  32.8 us (9%)
  matrix products  26.4 us (7%)
  starting transfers between devices  22.5 us (6%)
  between operations  13.5 us (4%)
  blocking collectives  8.71 us (2%)
  other arithmetic  6.53 us (2%)
    ppermute x7, waiting for transfers between devices, shards(): lax.ppermute(current, 'sp', [(i_2, (i_2 + 1) % size) for i_2 in range(siz...  191 us
    all_gather x1, waiting for transfers between devices, shards(): up_part = add_rows(lax.all_gather(w_up, 'sp', axis=0, tiled=True))  38.1 us
    reduce_scatter x1, waiting for transfers between devices, shards(): lax.psum_scatter(jnp.dot(hidden, down_full, preferred_element_type=jnp.fl...  29.5 us
    unnamed x37, local copies, waits for them, and re-layouts  24 us
    ppermute x3, starting transfers between devices, with_halo(): lax.ppermute(lax.slice_in_dim(block, block.shape[dim] - width, None, axis...  14.9 us
    dot_general x1, matrix products, shards(): jnp.dot(hidden, down_full, preferred_element_type=jnp.float32)  13.2 us
    all_to_all x1, blocking collectives, shards(): lax.all_to_all(attended, 'tp', split_axis=0, concat_axis=1, tiled=True)  8.71 us
    dot_general x1, matrix products, add_rows(): return jnp.dot(normed, piece, preferred_element_type=jnp.float32)  8.5 us
  transfers between devices with their start and end apart: 18, of which 10 were waited for; matrix products, arithmetic and copies ran while one was open for 12% of the time, Pallas kernels for 0%

profile of v1, /device:TPU:0, one launch (start us, length us, event | category | flops | bytes accessed | tf_op | source)
XLA Modules:
  0.0 372.6 jit_solution(8088962765178282125)
XLA Ops:
  8.1 1.3 collective-permute-start.3
  9.4 5.5 %collective-permute-start.2 = (s32[128]{0:T(128)S(1)}, s32[128]{0:T(128)S(1)}, u32[]{:S(2)}, u32[]{:S(2)}) collective-permute-start(s32[128]{0:T(128)S(1)} %get-tuple-element.16), channel_id=1, source_target_pairs={{0,4},{4,8},{8,12},{12,16},{16,20},{20,24},{24,28},{1,5},{5,9},{9,... | collective-permute-start | bytes 1544 | tf_op jit(solution)/shard_map/ppermute | solution.py:17
  15.7 4.8 %collective-permute-start.4 = (bf16[128,128]{1,0:T(8,128)(2,1)S(1)}, bf16[128,128]{1,0:T(8,128)(2,1)S(1)}, u32[]{:S(2)}, u32[]{:S(2)}) collective-permute-start(bf16[128,128]{1,0:T(8,128)(2,1)S(1)} %get-tuple-element.11), channel_id=1, source_target_pairs={{0,4},{4,8},{8,12},{12,16},{16,20},{20,24},{24,28},{1,5},{5,9},{9,... | collective-permute-start | bytes 98312 | tf_op jit(solution)/shard_map/ppermute | solution.py:17
  20.5 1.3 collective-permute-start.5
  22.6 4.5 %collective-permute-start = (bf16[128,128]{1,0:T(8,128)(2,1)S(1)}, bf16[128,128]{1,0:T(8,128)(2,1)S(1)}, u32[]{:S(2)}, u32[]{:S(2)}) collective-permute-start(bf16[128,128]{1,0:T(8,128)(2,1)S(1)} %get-tuple-element.7), channel_id=1, source_target_pairs={{0,4},{4,8},{8,12},{12,16},{16,20},{20,24},{24,28},{1,5},{5,9},{9,... | collective-permute-start | bytes 98312 | tf_op jit(solution)/shard_map/ppermute | solution.py:17
  27.1 1.0 reshape.90
  28.2 1.0 reshape.87
  29.4 1.2 reshape.92
  31.6 1.3 collective-permute-start.1
  36.2 1.2 collective-permute-done.1
  40.6 8.7 %all_to_all.19 = bf16[4,128,256]{1,2,0:T(8,128)(2,1)S(1)} all-to-all(bf16[4,128,256]{1,2,0:T(8,128)(2,1)S(1)} %bitcast.41), channel_id=1, replica_groups=mesh['sp'=8,'tp'=4] {'tp'}, dimensions={0} | all-to-all | bytes 524288 | tf_op jit(solution)/shard_map/all_to_all | solution.py:76
  49.3 3.0 multiply_reduce_fusion
  54.7 2.5 collective-permute-start.6
  57.2 17.8 %collective-permute-done.6 = bf16[1408,256]{1,0:T(8,128)(2,1)S(1)} collective-permute-done((bf16[1408,256]{1,0:T(8,128)(2,1)S(1)}, bf16[1408,256]{1,0:T(8,128)(2,1)S(1)}, u32[]{:S(2)}, u32[]{:S(2)}) %collective-permute-start.6) | collective-permute-done | bytes 720928 | tf_op jit(solution)/shard_map/ppermute | solution.py:90
  75.0 23.3 %collective-permute-done.7 = bf16[1408,256]{1,0:T(8,128)(2,1)S(1)} collective-permute-done((bf16[1408,256]{1,0:T(8,128)(2,1)S(1)}, bf16[1408,256]{1,0:T(8,128)(2,1)S(1)}, u32[]{:S(2)}, u32[]{:S(2)}) %collective-permute-start.7) | collective-permute-done | bytes 720928 | tf_op jit(solution)/shard_map/ppermute | solution.py:90
  98.2 35.0 %collective-permute-done.8 = bf16[1408,256]{1,0:T(8,128)(2,1)S(1)} collective-permute-done((bf16[1408,256]{1,0:T(8,128)(2,1)S(1)}, bf16[1408,256]{1,0:T(8,128)(2,1)S(1)}, u32[]{:S(2)}, u32[]{:S(2)}) %collective-permute-start.8) | collective-permute-done | bytes 720928 | tf_op jit(solution)/shard_map/ppermute | solution.py:90
  134.1 32.2 %collective-permute-done.9 = bf16[1408,256]{1,0:T(8,128)(2,1)S(1)} collective-permute-done((bf16[1408,256]{1,0:T(8,128)(2,1)S(1)}, bf16[1408,256]{1,0:T(8,128)(2,1)S(1)}, u32[]{:S(2)}, u32[]{:S(2)}) %collective-permute-start.9) | collective-permute-done | bytes 720928 | tf_op jit(solution)/shard_map/ppermute | solution.py:90
  167.2 34.3 %collective-permute-done.10 = bf16[1408,256]{1,0:T(8,128)(2,1)S(1)} collective-permute-done((bf16[1408,256]{1,0:T(8,128)(2,1)S(1)}, bf16[1408,256]{1,0:T(8,128)(2,1)S(1)}, u32[]{:S(2)}, u32[]{:S(2)}) %collective-permute-start.10) | collective-permute-done | bytes 720928 | tf_op jit(solution)/shard_map/ppermute | solution.py:90
  202.3 23.5 %collective-permute-done.11 = bf16[1408,256]{1,0:T(8,128)(2,1)} collective-permute-done((bf16[1408,256]{1,0:T(8,128)(2,1)S(1)}, bf16[1408,256]{1,0:T(8,128)(2,1)}, u32[]{:S(2)}, u32[]{:S(2)}) %collective-permute-start.11) | collective-permute-done | bytes 720928 | tf_op jit(solution)/shard_map/ppermute | solution.py:90
  225.8 1.1 collective-permute-start.12
  226.9 25.5 %collective-permute-done.12 = bf16[1408,256]{1,0:T(8,128)(2,1)} collective-permute-done((bf16[1408,256]{1,0:T(8,128)(2,1)}, bf16[1408,256]{1,0:T(8,128)(2,1)}, u32[]{:S(2)}, u32[]{:S(2)}) %collective-permute-start.12) | collective-permute-done | bytes 720928 | tf_op jit(solution)/shard_map/ppermute | solution.py:90
  252.4 2.1 constant_dynamic-update-slice_fusion.15
  254.5 2.1 constant_dynamic-update-slice_fusion.14
  256.6 2.2 constant_dynamic-update-slice_fusion.13
  258.8 2.2 constant_dynamic-update-slice_fusion.12
  264.8 2.1 constant_dynamic-update-slice_fusion.7
  266.9 2.1 constant_dynamic-update-slice_fusion.6
  274.8 8.5 %fusion.34 = f32[512,1408]{1,0:T(8,128)} fusion(bf16[512,2048]{1,0:T(8,128)(2,1)} %all-gather.7.cloned.1.call-done, bf16[2048,1408]{1,0:T(8,128)(2,1)} %all-gather.9.cloned.1.call-done), kind=kOutput, calls=%fused_computation.71 | convolution fusion | flops 2952790016 | bytes 10747904 | tf_op jit(solution)/shard_map/dot_general | solution.py:82
  283.3 38.1 %all-gather.11.cloned.1.call-done = bf16[2048,1408]{1,0:T(8,128)(2,1)} async-done(((bf16[256,1408]{1,0:T(8,128)(2,1)}), bf16[2048,1408]{1,0:T(8,128)(2,1)}) %all-gather.11.cloned.1.call-update) | async-done | bytes 5767184 | tf_op jit(solution)/shard_map/all_gather | solution.py:85
  321.4 13.2 %fusion.3 = bf16[512,2048]{1,0:T(8,128)(2,1)} fusion(bf16[1408,4096]{1,0:T(8,128)(2,1)} %constant_dynamic-update-slice_fusion, s32[]{:T(128)S(6)} %select_n.27, bf16[512,2048]{1,0:T(8,128)(2,1)S(1)} %copy-done.10, bf16[2048,1408]{1,0:T(8,128)(2,1)} %all-gather.11.cloned.1.call-done, f32[512,1408]{1,0:T(8,128)} %fusion.34), kind=kOutput, calls=%fused_computation.7 | convolution fusion | flops 5910953984 | bytes 18612228 | tf_op jit(solution)/shard_map/dot_general | solution.py:95
  334.6 29.5 %reduce-scatter.2.cloned.1.call-done = bf16[128,2048]{1,0:T(8,128)(2,1)} async-done(((bf16[512,2048]{1,0:T(8,128)(2,1)}), bf16[128,2048]{1,0:T(8,128)(2,1)}) %reduce-scatter.2.cloned.1.call-update) | async-done | bytes 524304 | tf_op jit(solution)/shard_map/reduce_scatter | solution.py:94
  364.1 1.9 add_convert_fusion
  (84 shorter events, 25.1 us)
Async XLA Ops:
  6.5 30.9 %copy-start.7 = (bf16[512,128]{1,0:T(8,128)(2,1)S(1)}, bf16[512,128]{1,0:T(8,128)(2,1)}, u32[]{:S(2)}) copy-start(bf16[512,128]{1,0:T(8,128)(2,1)} %param.13) | copy-start | bytes 393220
  6.5 42.8 %all-gather.5.cloned.1.call-start = ((), (), s32[]{:S(2)}) async-start(), calls=%async_computation.2 | async-start | bytes 5242880 | tf_op jit(solution)/shard_map/all_gather | solution.py:41
  7.3 267.5 %all-gather.7.cloned.1.call-start = ((), (), s32[]{:S(2)}) async-start(), calls=%async_computation.3 | async-start | bytes 2621440 | tf_op jit(solution)/shard_map/all_gather | solution.py:79
  8.1 23.6 %collective-permute-start.3 = (s32[128]{0:T(128)S(1)}, s32[128]{0:T(128)S(1)}, u32[]{:S(2)}, u32[]{:S(2)}) collective-permute-start(s32[128]{0:T(128)S(1)} %get-tuple-element.17), channel_id=1, source_target_pairs={{4,0},{8,4},{12,8},{16,12},{20,16},{24,20},{28,24},{5,1},{9,5},{13... | collective-permute-start | bytes 1544 | tf_op jit(solution)/shard_map/ppermute | solution.py:20
  9.4 23.6 %collective-permute-start.2 = (s32[128]{0:T(128)S(1)}, s32[128]{0:T(128)S(1)}, u32[]{:S(2)}, u32[]{:S(2)}) collective-permute-start(s32[128]{0:T(128)S(1)} %get-tuple-element.16), channel_id=1, source_target_pairs={{0,4},{4,8},{8,12},{12,16},{16,20},{20,24},{24,28},{1,5},{5,9},{9,... | collective-permute-start | bytes 1544 | tf_op jit(solution)/shard_map/ppermute | solution.py:17
  15.7 18.9 %collective-permute-start.4 = (bf16[128,128]{1,0:T(8,128)(2,1)S(1)}, bf16[128,128]{1,0:T(8,128)(2,1)S(1)}, u32[]{:S(2)}, u32[]{:S(2)}) collective-permute-start(bf16[128,128]{1,0:T(8,128)(2,1)S(1)} %get-tuple-element.11), channel_id=1, source_target_pairs={{0,4},{4,8},{8,12},{12,16},{16,20},{20,24},{24,28},{1,5},{5,9},{9,... | collective-permute-start | bytes 98312 | tf_op jit(solution)/shard_map/ppermute | solution.py:17
  20.5 14.1 %collective-permute-start.5 = (bf16[128,128]{1,0:T(8,128)(2,1)S(1)}, bf16[128,128]{1,0:T(8,128)(2,1)S(1)}, u32[]{:S(2)}, u32[]{:S(2)}) collective-permute-start(bf16[128,128]{1,0:T(8,128)(2,1)S(1)} %get-tuple-element.12), channel_id=1, source_target_pairs={{4,0},{8,4},{12,8},{16,12},{20,16},{24,20},{28,24},{5,1},{9,5},{13... | collective-permute-start | bytes 98312 | tf_op jit(solution)/shard_map/ppermute | solution.py:20
  22.6 13.6 %collective-permute-start = (bf16[128,128]{1,0:T(8,128)(2,1)S(1)}, bf16[128,128]{1,0:T(8,128)(2,1)S(1)}, u32[]{:S(2)}, u32[]{:S(2)}) collective-permute-start(bf16[128,128]{1,0:T(8,128)(2,1)S(1)} %get-tuple-element.7), channel_id=1, source_target_pairs={{0,4},{4,8},{8,12},{12,16},{16,20},{20,24},{24,28},{1,5},{5,9},{9,... | collective-permute-start | bytes 98312 | tf_op jit(solution)/shard_map/ppermute | solution.py:17
  31.6 5.8 %collective-permute-start.1 = (bf16[128,128]{1,0:T(8,128)(2,1)S(1)}, bf16[128,128]{1,0:T(8,128)(2,1)S(1)}, u32[]{:S(2)}, u32[]{:S(2)}) collective-permute-start(bf16[128,128]{1,0:T(8,128)(2,1)S(1)} %get-tuple-element.8), channel_id=1, source_target_pairs={{4,0},{8,4},{12,8},{16,12},{20,16},{24,20},{28,24},{5,1},{9,5},{13... | collective-permute-start | bytes 98312 | tf_op jit(solution)/shard_map/ppermute | solution.py:20
  39.6 9.7 %copy-start.8 = (bf16[128,2048]{1,0:T(8,128)(2,1)S(1)}, bf16[128,2048]{1,0:T(8,128)(2,1)}, u32[]{:S(2)}) copy-start(bf16[128,2048]{1,0:T(8,128)(2,1)} %param.16) | copy-start | bytes 1572868
  40.6 11.8 %copy-start.9 = (f32[2048]{0:T(1024)S(1)}, f32[2048]{0:T(1024)}, u32[]{:S(2)}) copy-start(f32[2048]{0:T(1024)} %param.18) | copy-start | bytes 24580
  40.6 14.1 %copy-start = (bf16[1408,256]{1,0:T(8,128)(2,1)S(1)}, bf16[1408,256]{1,0:T(8,128)(2,1)}, u32[]{:S(2)}) copy-start(bf16[1408,256]{1,0:T(8,128)(2,1)} %param.21) | copy-start | bytes 2162692
  53.3 221.5 %all-gather.9.cloned.1.call-start = ((), (), s32[]{:S(2)}) async-start(), calls=%async_computation.4 | async-start | bytes 6488064 | tf_op jit(solution)/shard_map/all_gather | solution.py:84
  54.1 267.3 %all-gather.11.cloned.1.call-start = ((), (), s32[]{:S(2)}) async-start(), calls=%async_computation.5 | async-start | bytes 6488064 | tf_op jit(solution)/shard_map/all_gather | solution.py:85
  54.6 309.5 %reduce-scatter.2.cloned.1.call-start = ((), (), s32[]{:S(2)}) async-start(), calls=%async_computation.6 | async-start | bytes 2621440 | tf_op jit(solution)/shard_map/reduce_scatter | solution.py:94
  54.7 20.3 %collective-permute-start.6 = (bf16[1408,256]{1,0:T(8,128)(2,1)S(1)}, bf16[1408,256]{1,0:T(8,128)(2,1)S(1)}, u32[]{:S(2)}, u32[]{:S(2)}) collective-permute-start(bf16[1408,256]{1,0:T(8,128)(2,1)S(1)} %copy-done), channel_id=1, source_target_pairs={{0,4},{4,8},{8,12},{12,16},{16,20},{20,24},{24,28},{28,0},{1,5},{5... | collective-permute-start | bytes 2162696 | tf_op jit(solution)/shard_map/ppermute | solution.py:90
  75.0 23.3 %collective-permute-start.7 = (bf16[1408,256]{1,0:T(8,128)(2,1)S(1)}, bf16[1408,256]{1,0:T(8,128)(2,1)S(1)}, u32[]{:S(2)}, u32[]{:S(2)}) collective-permute-start(bf16[1408,256]{1,0:T(8,128)(2,1)S(1)} %collective-permute-done.6), channel_id=1, source_target_pairs={{0,4},{4,8},{8,12},{12,16},{16,20},{20,24},{24,28},{28,0},{1,5},{5... | collective-permute-start | bytes 2162696 | tf_op jit(solution)/shard_map/ppermute | solution.py:90
  98.2 35.0 %collective-permute-start.8 = (bf16[1408,256]{1,0:T(8,128)(2,1)S(1)}, bf16[1408,256]{1,0:T(8,128)(2,1)S(1)}, u32[]{:S(2)}, u32[]{:S(2)}) collective-permute-start(bf16[1408,256]{1,0:T(8,128)(2,1)S(1)} %collective-permute-done.7), channel_id=1, source_target_pairs={{0,4},{4,8},{8,12},{12,16},{16,20},{20,24},{24,28},{28,0},{1,5},{5... | collective-permute-start | bytes 2162696 | tf_op jit(solution)/shard_map/ppermute | solution.py:90
  133.2 0.9 copy-start.1
  134.1 32.3 %collective-permute-start.9 = (bf16[1408,256]{1,0:T(8,128)(2,1)S(1)}, bf16[1408,256]{1,0:T(8,128)(2,1)S(1)}, u32[]{:S(2)}, u32[]{:S(2)}) collective-permute-start(bf16[1408,256]{1,0:T(8,128)(2,1)S(1)} %collective-permute-done.8), channel_id=1, source_target_pairs={{0,4},{4,8},{8,12},{12,16},{16,20},{20,24},{24,28},{28,0},{1,5},{5... | collective-permute-start | bytes 2162696 | tf_op jit(solution)/shard_map/ppermute | solution.py:90
  166.3 0.9 copy-start.3
  167.2 34.3 %collective-permute-start.10 = (bf16[1408,256]{1,0:T(8,128)(2,1)S(1)}, bf16[1408,256]{1,0:T(8,128)(2,1)S(1)}, u32[]{:S(2)}, u32[]{:S(2)}) collective-permute-start(bf16[1408,256]{1,0:T(8,128)(2,1)S(1)} %collective-permute-done.9), channel_id=1, source_target_pairs={{0,4},{4,8},{8,12},{12,16},{16,20},{20,24},{24,28},{28,0},{1,5},{5... | collective-permute-start | bytes 2162696 | tf_op jit(solution)/shard_map/ppermute | solution.py:90
  201.5 0.9 copy-start.5
  202.3 23.5 %collective-permute-start.11 = (bf16[1408,256]{1,0:T(8,128)(2,1)S(1)}, bf16[1408,256]{1,0:T(8,128)(2,1)}, u32[]{:S(2)}, u32[]{:S(2)}) collective-permute-start(bf16[1408,256]{1,0:T(8,128)(2,1)S(1)} %collective-permute-done.10), channel_id=1, source_target_pairs={{0,4},{4,8},{8,12},{12,16},{16,20},{20,24},{24,28},{28,0},{1,5},{5... | collective-permute-start | bytes 2162696 | tf_op jit(solution)/shard_map/ppermute | solution.py:90
  225.8 26.6 %collective-permute-start.12 = (bf16[1408,256]{1,0:T(8,128)(2,1)}, bf16[1408,256]{1,0:T(8,128)(2,1)}, u32[]{:S(2)}, u32[]{:S(2)}) collective-permute-start(bf16[1408,256]{1,0:T(8,128)(2,1)} %collective-permute-done.11), channel_id=1, source_target_pairs={{0,4},{4,8},{8,12},{12,16},{16,20},{20,24},{24,28},{28,0},{1,5},{5... | collective-permute-start | bytes 2162696 | tf_op jit(solution)/shard_map/ppermute | solution.py:90
  226.9 34.0 %copy-start.2 = (bf16[1408,256]{1,0:T(8,128)(2,1)S(1)}, bf16[1408,256]{1,0:T(8,128)(2,1)}, u32[]{:S(2)}) copy-start(bf16[1408,256]{1,0:T(8,128)(2,1)} %copy-done.1) | copy-start | bytes 2162692
  256.6 12.4 %copy-start.6 = (bf16[1408,256]{1,0:T(8,128)(2,1)S(1)}, bf16[1408,256]{1,0:T(8,128)(2,1)}, u32[]{:S(2)}) copy-start(bf16[1408,256]{1,0:T(8,128)(2,1)} %copy-done.5) | copy-start | bytes 2162692
  258.8 11.2 %copy-start.4 = (bf16[1408,256]{1,0:T(8,128)(2,1)S(1)}, bf16[1408,256]{1,0:T(8,128)(2,1)}, u32[]{:S(2)}) copy-start(bf16[1408,256]{1,0:T(8,128)(2,1)} %copy-done.3) | copy-start | bytes 2162692
  274.8 46.6 %copy-start.10 = (bf16[512,2048]{1,0:T(8,128)(2,1)S(1)}, bf16[512,2048]{1,0:T(8,128)(2,1)}, u32[]{:S(2)}) copy-start(bf16[512,2048]{1,0:T(8,128)(2,1)} %all-gather.7.cloned.1.call-done) | copy-start | bytes 6291460
Sparse Core Ops, SparseCore 0:
  8.9 37.1 all-gather.4
  53.4 22.7 all-gather.6
  78.4 132.7 all-gather.8
  213.2 108.1 all-gather.10
  334.8 29.3 reduce-scatter.1
